TPU v7x, 32 devices: a whole 2x2x4 slice. The times are simulated.
32 devices in a mesh: rep: 4 (over z), fs: 4 (over y, x), tp: 2 (over core).
Axes of the slice: x: 2, y: 2, z: 4, core: 2. Of those that a mesh axis runs over, the one named last changes fastest.
Arguments:
- residual: bfloat16 [16, 256, 2048], P(('rep', 'fs'), None, 'tp'), may hold values from -6 to 6
- queries: bfloat16 [16, 256, 2048], P(('rep', 'fs'), None, 'tp'), may hold values from -6 to 6
- key_matrix: bfloat16 [16, 256, 2048], P(('rep', 'fs'), None, 'tp'), may hold values from -6 to 6
- value_matrix: bfloat16 [16, 256, 2048], P(('rep', 'fs'), None, 'tp'), may hold values from -6 to 6
- decay_logodds: float32 [16, 256, 2048], P(('rep', 'fs'), None, 'tp'), may hold values from -3.4 to 8.9, as said below
- decay_surge: float32 [16, 256, 8], P(('rep', 'fs'), None, 'tp'), may hold values from -2.1 to 0, as said below
- head_norm_gain: float32 [256], replicated, may hold values from 0.1 to 1.9
- output_matrix: float32 [2048, 2048], P('fs', 'tp'), may hold values from -0.125 to 0.125
- output_column_scale: float32 [2048], P('tp'), may hold values from 0.5 to 2
- premix_norm_gain: float32 [2048], replicated, may hold values from 0.1 to 1.9
- gate_matrix: float32 [2048, 2816], P('fs', 'tp'), may hold values from -0.125 to 0.125
- gate_column_scale: float32 [2816], P('tp'), may hold values from 0.5 to 2
- up_matrix: float32 [2048, 2816], P('fs', 'tp'), may hold values from -0.125 to 0.125
- up_column_scale: float32 [2816], P('tp'), may hold values from 0.5 to 2
- down_matrix: float32 [2048, 2816], P('fs', 'tp'), may hold values from -0.109375 to 0.109375
- down_column_scale: float32 [2048], P('tp'), may hold values from 0.5 to 2
Outputs:
- layer_out: bfloat16 [16, 256, 2048], P(('rep', 'fs'), None, 'tp')
Inputs may be any that keep to these rules, and one draw needn't show every extreme that they name: `decay_logodds`: log-odds of a key channel's decay. `decay_surge`: non-positive log-factors of a head's state.
All inputs are finite; a program needn't handle non-finite values.
Results may differ from a plain program's by a relative error of at most 0.018.
Values may be sent and summed in bfloat16 or wider, within the bound.
No kernel may reach another device: no remote copies, remote signals or barrier semaphores. Data moves between devices by JAX's collectives and lax.ppermute only.
A program may use at most 128 MiB of HBM per device.

v0:
```python
import jax
import jax.numpy as jnp
from jax import lax
from jax.sharding import PartitionSpec as P

BLOCK = 64


epsilon = 1e-06
softness_factor = 16.0
highest = lax.Precision.HIGHEST


def one_direction(query_heads, key_heads, value_heads, log_decay_values):
    sequence_batch, head_total, token_length, key_channel_width = query_heads.shape
    value_width = value_heads.shape[-1]
    block_count = token_length // BLOCK

    def blocks(tensor):
        return tensor.reshape(sequence_batch, head_total, block_count, BLOCK, tensor.shape[-1])

    q_blocks = blocks(query_heads)
    k_blocks = blocks(key_heads)
    v_blocks = blocks(value_heads)
    running = jnp.cumsum(blocks(log_decay_values), axis=3)
    block_end = running[:, :, :, -1:, :]
    q_dec = q_blocks * jnp.exp(running)
    k_inv = k_blocks * jnp.exp(-running)
    k_end = k_blocks * jnp.exp(block_end - running)
    lower_mask = jnp.tril(jnp.ones((BLOCK, BLOCK), jnp.float32))
    scores = jnp.einsum("shnid,shnjd->shnij", q_dec, k_inv, precision=highest) * lower_mask
    inner_part = jnp.einsum("shnij,shnje->shnie", scores, v_blocks, precision=highest)
    fading = jnp.exp(block_end[:, :, :, 0, :])

    def advance(memory, pieces):
        q_piece, k_piece, v_piece, f_piece = pieces
        carried = jnp.einsum("shcd,shde->shce", q_piece, memory, precision=highest)
        memory = f_piece[..., None] * memory + jnp.einsum(
            "shcd,shce->shde", k_piece, v_piece, precision=highest
        )
        return (memory, carried)

    pieces = tuple((jnp.moveaxis(tensor, 2, 0) for tensor in (q_dec, k_end, v_blocks, fading)))
    initial = jnp.zeros((sequence_batch, head_total, key_channel_width, value_width), jnp.float32)
    _, carried = lax.scan(advance, initial, pieces)
    summed = inner_part + jnp.moveaxis(carried, 0, 2)
    return summed.reshape(sequence_batch, head_total, token_length, value_width)


def backwards(tensor):
    return tensor[:, :, ::-1]


def linear_attend(queries, key_matrix, value_matrix, decay_logodds, decay_surge, head_norm_gain):
    sequence_batch, token_length, head_total = decay_surge.shape
    key_channel_width = queries.shape[-1] // head_total
    value_width = value_matrix.shape[-1] // head_total

    def split_heads(tensor, width):
        return jnp.transpose(
            tensor.astype(jnp.float32).reshape(sequence_batch, token_length, head_total, width),
            (0, 2, 1, 3),
        )

    query_heads = split_heads(queries, key_channel_width) * key_channel_width ** (-0.5)
    key_heads = split_heads(key_matrix, key_channel_width)
    value_heads = split_heads(value_matrix, value_width)
    gate_values = (
        jax.nn.log_sigmoid(decay_logodds).reshape(
            sequence_batch, token_length, head_total, key_channel_width
        )
        / softness_factor
    )
    log_decay_values = jnp.transpose(gate_values + decay_surge[..., None], (0, 2, 1, 3))
    forward = one_direction(query_heads, key_heads, value_heads, log_decay_values)
    backward = backwards(
        one_direction(
            backwards(query_heads),
            backwards(key_heads),
            backwards(value_heads),
            backwards(log_decay_values),
        )
    )
    attended = forward + backward
    scaled = (
        attended
        * lax.rsqrt(jnp.mean(attended * attended, axis=-1, keepdims=True) + epsilon)
        * head_norm_gain
    )
    merged = jnp.transpose(scaled, (0, 2, 1, 3)).reshape(
        sequence_batch * token_length, head_total * value_width
    )
    return merged.astype(jnp.bfloat16)


def by_rows(left, right):
    return lax.dot_general(
        left, right, (((1,), (1,)), ((), ())), preferred_element_type=jnp.float32
    )


def body(
    residual,
    queries,
    key_matrix,
    value_matrix,
    decay_logodds,
    decay_surge,
    head_norm_gain,
    output_matrix,
    output_column_scale,
    premix_norm_gain,
    gate_matrix,
    gate_column_scale,
    up_matrix,
    up_column_scale,
    down_matrix,
    down_column_scale,
):
    sequence_batch, token_length, local_width = residual.shape
    row_count = sequence_batch * token_length
    normalized_rows = linear_attend(
        queries, key_matrix, value_matrix, decay_logodds, decay_surge, head_norm_gain
    )
    out_half = output_matrix.astype(jnp.bfloat16)
    out_full = lax.all_gather(out_half, "fs", axis=0, tiled=True)
    mix_terms = by_rows(normalized_rows, out_full)
    mix_total = lax.psum_scatter(
        mix_terms.astype(jnp.bfloat16), "tp", scatter_dimension=1, tiled=True
    ).astype(jnp.float32)
    own_rows = residual.reshape(row_count, local_width).astype(jnp.float32)
    updated = (own_rows + output_column_scale * mix_total).astype(jnp.bfloat16)
    features = lax.all_gather(updated, "tp", axis=1, tiled=True)
    wide_rows = features.astype(jnp.float32)
    factor = lax.rsqrt(jnp.mean(wide_rows * wide_rows, axis=-1, keepdims=True) + epsilon)
    normin = (wide_rows * factor * premix_norm_gain).astype(jnp.bfloat16)
    gate_half = gate_matrix.astype(jnp.bfloat16)
    up_half = up_matrix.astype(jnp.bfloat16)
    down_half = down_matrix.astype(jnp.bfloat16)
    gate_full, up_full, down_full = (
        lax.all_gather(gate_half, "fs", axis=0, tiled=True),
        lax.all_gather(up_half, "fs", axis=0, tiled=True),
        lax.all_gather(down_half, "fs", axis=0, tiled=True),
    )
    gate_pre = jnp.dot(normin, gate_full, preferred_element_type=jnp.float32)
    up_pre = jnp.dot(normin, up_full, preferred_element_type=jnp.float32)
    hidden = (jax.nn.silu(gate_pre * gate_column_scale) * (up_pre * up_column_scale)).astype(
        jnp.bfloat16
    )
    down_terms = by_rows(hidden, down_full)
    down_total = lax.psum_scatter(
        down_terms.astype(jnp.bfloat16), "tp", scatter_dimension=1, tiled=True
    ).astype(jnp.float32)
    result = (updated.astype(jnp.float32) + down_column_scale * down_total).astype(jnp.bfloat16)
    return result.reshape(sequence_batch, token_length, local_width)


def solution(mesh):
    return jax.shard_map(
        body,
        mesh=mesh,
        in_specs=(
            P(("rep", "fs"), None, "tp"),
            P(("rep", "fs"), None, "tp"),
            P(("rep", "fs"), None, "tp"),
            P(("rep", "fs"), None, "tp"),
            P(("rep", "fs"), None, "tp"),
            P(("rep", "fs"), None, "tp"),
            P(),
            P("fs", "tp"),
            P("tp"),
            P(),
            P("fs", "tp"),
            P("tp"),
            P("fs", "tp"),
            P("tp"),
            P("fs", "tp"),
            P("tp"),
        ),
        out_specs=P(("rep", "fs"), None, "tp"),
        check_vma=False,
    )
```

profile of v0, /device:TPU:0, one launch (start us, length us, event | category | flops | bytes accessed | tf_op | source)
XLA Modules:
  0.0 382.0 jit_solution(15835709176157356482)
XLA Ops:
  6.5 2.8 convert_element_type.65
  9.5 0.6 fusion.38
  10.1 0.5 div.26
  10.8 0.3 add_bitcast_fusion
  11.3 1.2 copy.83
  12.5 4.4 %reduce_window_sum.18 = f32[1,4,4,64,256]{4,3,2,1,0:T(8,128)S(1)} reduce-window(f32[1,4,4,64,256]{4,3,2,1,0:T(8,128)} %bitcast.221, f32[]{:T(128)} %constant.50.clone.1), window={size=1x1x1x64x1 pad=0_0x0_0x0_0x63_0x0_0}, to_apply=%region_3.4 | reduce-window | flops 16515072 | bytes 2097156 | tf_op jit(solution)/shard_map/jit(cumsum)/reduce_window_sum | solution.py:25
  17.2 5.2 %rev.17 = f32[1,4,256,256]{3,2,1,0:T(8,128)} reverse(f32[1,4,256,256]{3,2,1,0:T(8,128)S(1)} %bitcast.201), dimensions={2} | reverse | bytes 2097152 | tf_op jit(solution)/shard_map/rev | solution.py:51
  22.5 1.1 transpose.94
  23.6 1.0 copy-done.1
  24.6 1.1 copy.125
  25.7 8.9 %reverse.3 = f32[1,4,256,256]{3,2,1,0:T(8,128)} reverse(f32[1,4,256,256]{3,2,1,0:T(8,128)} %bitcast.223), dimensions={2} | reverse | bytes 2097152 | tf_op jit(solution)/shard_map/reverse
  34.6 2.3 broadcast_multiply_fusion
  36.9 2.0 copy.75
  39.0 8.8 %rev.18 = f32[1,4,256,256]{2,3,1,0:T(8,128)} reverse(bf16[1,4,256,256]{2,3,1,0:T(8,128)(2,1)} %bitcast.214), dimensions={2} | reverse | bytes 1572864 | tf_op jit(solution)/shard_map/rev | solution.py:51
  47.8 2.6 copy.84
  50.4 3.3 multiply_bitcast_fusion
  53.7 1.1 broadcast.94.clone2.1
  54.8 19.1 %while.27 = (s32[]{:T(128)}, f32[1,4,256,256]{3,2,1,0:T(8,128)S(1)}, f32[4,1,4,64,256]{4,3,0,2,1:T(8,128)}, f32[4,1,4,256]{3,1,0,2:T(1,128)S(1)}, f32[4,1,4,64,2...) while((s32[]{:T(128)}, ...), condition=%wide.region_5.6_spmd.clone, body=%wide.region_4.5_spmd.clone.sunk | while | flops 403701760 | bytes 4216940 | solution.py:45
  54.8 2.5 fusion.87
  57.3 2.3 fusion.86
  59.6 2.5 fusion.87
  62.0 2.3 fusion.86
  64.3 2.5 fusion.87
  66.8 2.3 fusion.86
  69.1 2.5 fusion.87
  71.6 2.3 fusion.86
  73.9 2.5 copy.73
  76.4 1.3 copy.77
  77.7 2.1 copy.76
  79.8 3.0 convolution_multiply_fusion.2
  82.8 1.1 fusion.36
  83.9 1.4 copy.91
  85.3 9.4 %rev.19 = f32[1,4,256,256]{2,3,1,0:T(8,128)} reverse(f32[1,4,256,256]{2,3,1,0:T(8,128)} %copy.91), dimensions={2} | reverse | bytes 2097152 | tf_op jit(solution)/shard_map/rev | solution.py:51
  94.7 4.4 %reduce_window_sum.17 = f32[1,4,4,64,256]{4,3,2,1,0:T(8,128)S(1)} reduce-window(f32[1,4,4,64,256]{4,3,2,1,0:T(8,128)} %bitcast.220, f32[]{:T(128)} %constant.50.clone.1), window={size=1x1x1x64x1 pad=0_0x0_0x0_0x63_0x0_0}, to_apply=%region_0.1 | reduce-window | flops 16515072 | bytes 2097156 | tf_op jit(solution)/shard_map/jit(cumsum)/reduce_window_sum | solution.py:25
  99.1 1.3 broadcast_multiply_fusion.1
  100.4 2.2 convolution_multiply_fusion.3
  102.6 1.7 multiply_bitcast_fusion.2
  104.4 16.6 %while.26 = (s32[]{:T(128)}, f32[1,4,256,256]{3,2,1,0:T(8,128)S(1)}, f32[4,1,4,64,256]{4,3,0,2,1:T(8,128)S(1)}, f32[4,1,4,256]{3,1,0,2:T(1,128)S(1)}, f32[4,1,4,...) while((s32[]{:T(128)}, ...), condition=%wide.region_2.3_spmd.clone, body=%wide.region_1.2_spmd.clone.sunk | while | flops 403701760 | bytes 4216940 | solution.py:45
  104.6 1.8 fusion.81
  106.4 2.3 fusion.80
  108.7 1.7 fusion.81
  110.5 2.3 fusion.80
  112.8 1.8 fusion.81
  114.5 2.3 fusion.80
  116.9 1.7 fusion.81
  118.6 2.3 fusion.80
  121.0 1.8 fusion.35
  122.8 0.3 copy.92
  123.3 0.5 copy-done.16
  124.0 4.6 %convolution_convert_fusion = bf16[256,2048]{1,0:T(8,128)(2,1)} fusion(bf16[256,1024]{0,1:T(8,128)(2,1)S(1)} %bitcast.225, bf16[2048,1024]{1,0:T(8,128)(2,1)} %all-gather.6.cloned.1.call-done), kind=kOutput, calls=%fused_computation.44 | convolution fusion | flops 1074266112 | bytes 5767168 | tf_op jit(solution)/shard_map/dot_general | solution.py:97
  128.6 11.2 %reduce-scatter.3.cloned.1.call-done = bf16[256,1024]{1,0:T(8,128)(2,1)} async-done(((bf16[256,2048]{1,0:T(8,128)(2,1)}), bf16[256,1024]{1,0:T(8,128)(2,1)}) %reduce-scatter.3.cloned.1.call-update) | async-done | bytes 524304 | tf_op jit(solution)/shard_map/reduce_scatter | solution.py:128
  139.9 2.0 fusion.39
  142.0 1.3 convert_element_type.72
  143.4 3.2 convert_element_type.73
  146.7 1.2 convert_element_type.75
  148.0 4.3 %all-gather.8.cloned.1.call-done = bf16[256,2048]{1,0:T(8,128)(2,1)} async-done(((bf16[256,1024]{1,0:T(8,128)(2,1)}), bf16[256,2048]{1,0:T(8,128)(2,1)}) %all-gather.8.cloned.1.call-update) | async-done | bytes 1048592 | tf_op jit(solution)/shard_map/all_gather | solution.py:133
  152.3 1.5 fusion.32
  153.8 67.0 %all-gather.10.cloned.1.call-done = bf16[2048,1408]{1,0:T(8,128)(2,1)} async-done(((bf16[512,1408]{1,0:T(8,128)(2,1)}), bf16[2048,1408]{1,0:T(8,128)(2,1)}) %all-gather.10.cloned.1.call-update) | async-done | bytes 5767184 | tf_op jit(solution)/shard_map/all_gather | solution.py:141
  220.8 4.8 %convolution_multiply_fusion.1 = f32[256,1408]{1,0:T(8,128)S(1)} fusion(bf16[2048,1408]{1,0:T(8,128)(2,1)} %all-gather.10.cloned.1.call-done, f32[1408]{0:T(1024)S(1)} %copy-done.17, bf16[256,2048]{1,0:T(8,128)(2,1)} %all-gather.8.cloned.1.call-done, f32[2048]{0:T(1024)S(1)} %copy-done.18, f32[256]{0:T(256)S(1)} %add_rsqrt_fusion.1), kind=kOutput, calls=%fused_computation.41 | convolution fusion | flops 1478852608 | bytes 8272384 | tf_op jit(solution)/shard_map/dot_general | solution.py:145
  225.7 62.5 %all-gather.12.cloned.1.call-done = bf16[2048,1408]{1,0:T(8,128)(2,1)} async-done(((bf16[512,1408]{1,0:T(8,128)(2,1)}), bf16[2048,1408]{1,0:T(8,128)(2,1)}) %all-gather.12.cloned.1.call-update) | async-done | bytes 5767184 | tf_op jit(solution)/shard_map/all_gather | solution.py:142
  288.2 67.4 %all-gather.14.cloned.1.call-done = bf16[2048,1408]{1,0:T(8,128)(2,1)} async-done(((bf16[512,1408]{1,0:T(8,128)(2,1)}), bf16[2048,1408]{1,0:T(8,128)(2,1)}) %all-gather.14.cloned.1.call-update) | async-done | bytes 5767184 | tf_op jit(solution)/shard_map/all_gather | solution.py:143
  355.6 8.9 %convolution_convert_fusion.1 = bf16[256,2048]{1,0:T(8,128)(2,1)} fusion(bf16[2048,1408]{1,0:T(8,128)(2,1)} %all-gather.14.cloned.1.call-done, bf16[2048,1408]{1,0:T(8,128)(2,1)} %all-gather.12.cloned.1.call-done, f32[256,1408]{1,0:T(8,128)S(1)} %convolution_multiply_fusion.1, f32[1408]{0:T(1024)S(1)} %copy-done.19, bf16[256,2048]{1,0:T(8,128)(2,1)S(1)} %copy-done.9, ...), kind=kOutput, calls=%fused_computation.46 | convolution fusion | flops 2957934592 | bytes 15088128 | tf_op jit(solution)/shard_map/dot_general | solution.py:97
  364.6 8.6 %reduce-scatter.5.cloned.1.call-done = bf16[256,1024]{1,0:T(8,128)(2,1)} async-done(((bf16[256,2048]{1,0:T(8,128)(2,1)}), bf16[256,1024]{1,0:T(8,128)(2,1)}) %reduce-scatter.5.cloned.1.call-update) | async-done | bytes 524304 | tf_op jit(solution)/shard_map/reduce_scatter | solution.py:151
  373.2 2.0 fusion.46
  (85 shorter events, 1.5 us)
Async XLA Ops:
  6.5 2.9 copy-start.10
  6.5 117.4 %all-gather.6.cloned.1.call-start = ((), (), s32[]{:S(2)}) async-start(), calls=%async_computation.2 | async-start | bytes 5242880 | tf_op jit(solution)/shard_map/all_gather | solution.py:126
  9.4 130.4 %reduce-scatter.3.cloned.1.call-start = ((), (), s32[]{:S(2)}) async-start(), calls=%async_computation.3 | async-start | bytes 1572864 | tf_op jit(solution)/shard_map/reduce_scatter | solution.py:128
  9.5 1.1 copy-start.15
  11.1 1.4 copy-start.2
  12.5 4.5 %copy-start.11 = (bf16[1,256,1024]{2,1,0:T(8,128)(2,1)S(1)}, bf16[1,256,1024]{2,1,0:T(8,128)(2,1)}, u32[]{:S(2)}) copy-start(bf16[1,256,1024]{2,1,0:T(8,128)(2,1)} %param.22) | copy-start | bytes 1572868
  23.6 1.0 copy-start.1
  73.9 2.5 copy-start.3
  79.8 3.0 copy-start
  79.8 3.1 copy-start.5
  120.9 2.2 copy-start.6
  123.1 0.7 copy-start.16
  124.0 15.9 %copy-start.12 = (bf16[1,256,1024]{2,1,0:T(8,128)(2,1)S(1)}, bf16[1,256,1024]{2,1,0:T(8,128)(2,1)}, u32[]{:S(2)}) copy-start(bf16[1,256,1024]{2,1,0:T(8,128)(2,1)} %param.20) | copy-start | bytes 1572868
  124.0 15.9 %copy-start.13 = (f32[1024]{0:T(1024)S(1)}, f32[1024]{0:T(1024)}, u32[]{:S(2)}) copy-start(f32[1024]{0:T(1024)} %param.28) | copy-start | bytes 12292
  128.6 13.4 %copy-start.7 = (f32[512,1408]{1,0:T(8,128)S(1)}, f32[512,1408]{1,0:T(8,128)}, u32[]{:S(2)}) copy-start(f32[512,1408]{1,0:T(8,128)} %param.30) | copy-start | bytes 8650756
  128.6 23.7 %all-gather.8.cloned.1.call-start = ((), (), s32[]{:S(2)}) async-start(), calls=%async_computation.4 | async-start | bytes 1572864 | tf_op jit(solution)/shard_map/all_gather | solution.py:133
  141.9 78.9 %all-gather.10.cloned.1.call-start = ((), (), s32[]{:S(2)}) async-start(), calls=%async_computation.5 | async-start | bytes 7208960 | tf_op jit(solution)/shard_map/all_gather | solution.py:141
  143.3 3.4 copy-start.8
  143.3 144.9 %all-gather.12.cloned.1.call-start = ((), (), s32[]{:S(2)}) async-start(), calls=%async_computation.6 | async-start | bytes 7208960 | tf_op jit(solution)/shard_map/all_gather | solution.py:142
  146.6 209.0 %all-gather.14.cloned.1.call-start = ((), (), s32[]{:S(2)}) async-start(), calls=%async_computation.7 | async-start | bytes 7208960 | tf_op jit(solution)/shard_map/all_gather | solution.py:143
  147.9 72.9 %copy-start.17 = (f32[1408]{0:T(1024)S(1)}, f32[1408]{0:T(1024)}, u32[]{:S(2)}) copy-start(f32[1408]{0:T(1024)} %param.31) | copy-start | bytes 16900
  147.9 72.9 %copy-start.18 = (f32[2048]{0:T(1024)S(1)}, f32[2048]{0:T(1024)}, u32[]{:S(2)}) copy-start(f32[2048]{0:T(1024)} %param.29) | copy-start | bytes 24580
  147.9 225.2 %reduce-scatter.5.cloned.1.call-start = ((), (), s32[]{:S(2)}) async-start(), calls=%async_computation.8 | async-start | bytes 1572864 | tf_op jit(solution)/shard_map/reduce_scatter | solution.py:151
  153.8 201.8 %copy-start.9 = (bf16[256,2048]{1,0:T(8,128)(2,1)S(1)}, bf16[256,2048]{1,0:T(8,128)(2,1)}, u32[]{:S(2)}) copy-start(bf16[256,2048]{1,0:T(8,128)(2,1)} %all-gather.8.cloned.1.call-done) | copy-start | bytes 3145732
  153.8 201.8 %copy-start.19 = (f32[1408]{0:T(1024)S(1)}, f32[1408]{0:T(1024)}, u32[]{:S(2)}) copy-start(f32[1408]{0:T(1024)} %param.33) | copy-start | bytes 16900
  225.7 147.5 %copy-start.4 = (bf16[256,1024]{1,0:T(8,128)(2,1)S(1)}, bf16[256,1024]{1,0:T(8,128)(2,1)}, u32[]{:S(2)}) copy-start(bf16[256,1024]{1,0:T(8,128)(2,1)} %fusion.39) | copy-start | bytes 1572868
  225.7 147.5 %copy-start.14 = (f32[1024]{0:T(1024)S(1)}, f32[1024]{0:T(1024)}, u32[]{:S(2)}) copy-start(f32[1024]{0:T(1024)} %param.35) | copy-start | bytes 12292
Sparse Core Ops, SparseCore 0:
  9.5 55.2 all-gather.5
  128.7 11.1 reduce-scatter.2
  142.0 10.1 all-gather.7
  154.0 66.8 all-gather.9
  222.5 65.6 all-gather.11
  289.9 65.6 all-gather.13
  364.7 8.3 reduce-scatter.4
where the time goes:
time: 385 us; the launch traced here: 382 us
  waiting for transfers between devices  221 us (57%)
  matrix products  61.5 us (16%)
  local copies, waits for them, and re-layouts  50.7 us (13%)
  other arithmetic  34.1 us (9%)
  between operations  13.9 us (4%)
    all_gather x1, waiting for transfers between devices, body(): lax.all_gather(down_half, 'fs', axis=0, tiled=True)  67.4 us
    all_gather x1, waiting for transfers between devices, body(): lax.all_gather(gate_half, 'fs', axis=0, tiled=True)  67 us
    all_gather x1, waiting for transfers between devices, body(): lax.all_gather(up_half, 'fs', axis=0, tiled=True)  62.5 us
    rev x6, local copies, waits for them, and re-layouts, backwards(): return tensor[:, :, ::-1]  27.4 us
    dot_general x8, matrix products, advance(): jnp.einsum('shcd,shce->shde', k_piece, v_piece, precision=highest)  18.3 us
    dot_general x8, matrix products, advance(): carried = jnp.einsum('shcd,shde->shce', q_piece, memory, precision=highest)  16.9 us
    dot_general x2, matrix products, by_rows(): lax.dot_general(left, right, (((1,), (1,)), ((), ())), preferred_element_...  13.5 us
    reduce_scatter x1, waiting for transfers between devices, body(): lax.psum_scatter(mix_terms.astype(jnp.bfloat16), 'tp', scatter_dimension=...  11.2 us
  transfers between devices with their start and end apart: 7, of which 6 were waited for; matrix products, arithmetic and copies ran while one was open for 33% of the time, Pallas kernels for 0%

commit v1 on v0

v1 whole, which is shorter than its diff:
```python
import functools

import jax
import jax.numpy as jnp
from jax import lax
from jax.experimental import pallas as pl
from jax.experimental.pallas import tpu as pltpu
from jax.sharding import PartitionSpec as P

BLOCK = 64

epsilon = 1e-06
softness_factor = 16.0
bf16 = jnp.bfloat16
f32 = jnp.float32


def attend_kernel(q_ref, k_ref, v_ref, odds_ref, surge_ref, gain_ref, out_ref):
    head = pl.program_id(1)
    tokens, width = q_ref.shape[1:]
    count = tokens // BLOCK
    surge_all = surge_ref[0]
    column = lax.broadcasted_iota(jnp.int32, surge_all.shape, 1)
    surge = jnp.sum(jnp.where(column == head, surge_all, 0.0), axis=1, keepdims=True)
    odds = odds_ref[0]
    log_decay = (jnp.minimum(odds, 0.0) - jnp.log1p(jnp.exp(-jnp.abs(odds)))) / softness_factor + surge
    row = lax.broadcasted_iota(jnp.int32, (BLOCK, BLOCK), 0)
    col = lax.broadcasted_iota(jnp.int32, (BLOCK, BLOCK), 1)
    lower = row >= col
    upper = row <= col
    tri = jnp.where(lower, 1.0, 0.0)

    def cut(tensor, n):
        return tensor[n * BLOCK : (n + 1) * BLOCK]

    query = q_ref[0].astype(f32) * width ** (-0.5)
    key = k_ref[0].astype(f32)
    value = v_ref[0]
    q_fwd, q_bwd, k_diag_f, k_diag_b, k_end, k_begin, total = [], [], [], [], [], [], []
    for n in range(count):
        step = cut(log_decay, n)
        running = lax.dot_general(
            tri, step, (((1,), (0,)), ((), ())), precision=lax.Precision.HIGHEST, preferred_element_type=f32
        )
        whole = running[BLOCK - 1 :, :]
        before = running - step
        after = whole - before
        q_n, k_n = cut(query, n), cut(key, n)
        q_fwd.append((q_n * jnp.exp(running)).astype(bf16))
        q_bwd.append((q_n * jnp.exp(after)).astype(bf16))
        k_diag_f.append((k_n * jnp.exp(-running)).astype(bf16))
        k_diag_b.append((k_n * jnp.exp(-after)).astype(bf16))
        k_end.append(k_n * jnp.exp(whole - running))
        k_begin.append(k_n * jnp.exp(before))
        total.append(jnp.exp(whole))

    def scores(left, right):
        return lax.dot_general(left, right, (((1,), (1,)), ((), ())), preferred_element_type=f32)

    gain = gain_ref[...]
    for n in range(count):
        fwd_keys, fade = [], None
        for m in range(n - 1, -1, -1):
            piece = k_end[m] if fade is None else k_end[m] * fade
            fwd_keys.insert(0, piece.astype(bf16))
            fade = total[m] if fade is None else fade * total[m]
        bwd_keys, fade = [], None
        for m in range(n + 1, count):
            piece = k_begin[m] if fade is None else k_begin[m] * fade
            bwd_keys.append(piece.astype(bf16))
            fade = total[m] if fade is None else fade * total[m]
        fwd = scores(q_fwd[n], jnp.concatenate(fwd_keys + [k_diag_f[n]], axis=0))
        bwd = scores(q_bwd[n], jnp.concatenate([k_diag_b[n]] + bwd_keys, axis=0))
        own = jnp.where(lower, fwd[:, n * BLOCK :], 0.0) + jnp.where(upper, bwd[:, :BLOCK], 0.0)
        pieces = []
        if n > 0:
            pieces.append(fwd[:, : n * BLOCK])
        pieces.append(own)
        if n < count - 1:
            pieces.append(bwd[:, BLOCK:])
        line = jnp.concatenate(pieces, axis=1).astype(bf16)
        attended = jnp.dot(line, value, preferred_element_type=f32)
        factor = lax.rsqrt(jnp.mean(attended * attended, axis=-1, keepdims=True) + epsilon)
        out_ref[0, n * BLOCK : (n + 1) * BLOCK, :] = (attended * factor * gain).astype(bf16)


def linear_attend(queries, key_matrix, value_matrix, decay_logodds, decay_surge, head_norm_gain):
    sequences, tokens, heads = decay_surge.shape
    key_width = queries.shape[-1] // heads
    value_width = value_matrix.shape[-1] // heads

    def spec(width):
        return pl.BlockSpec((1, tokens, width), lambda s, h: (s, 0, h))

    return pl.pallas_call(
        attend_kernel,
        grid=(sequences, heads),
        in_specs=[
            spec(key_width),
            spec(key_width),
            spec(value_width),
            spec(key_width),
            pl.BlockSpec((1, tokens, heads), lambda s, h: (s, 0, 0)),
            pl.BlockSpec((1, value_width), lambda s, h: (0, 0)),
        ],
        out_specs=spec(value_width),
        out_shape=jax.ShapeDtypeStruct((sequences, tokens, heads * value_width), bf16),
        compiler_params=pltpu.CompilerParams(dimension_semantics=("arbitrary", "arbitrary")),
        name="attend",
    )(queries, key_matrix, value_matrix, decay_logodds, decay_surge, head_norm_gain.reshape(1, -1))


def by_rows(left, right):
    return lax.dot_general(left, right, (((1,), (1,)), ((), ())), preferred_element_type=f32)


def body(
    residual,
    queries,
    key_matrix,
    value_matrix,
    decay_logodds,
    decay_surge,
    head_norm_gain,
    output_matrix,
    output_column_scale,
    premix_norm_gain,
    gate_matrix,
    gate_column_scale,
    up_matrix,
    up_column_scale,
    down_matrix,
    down_column_scale,
):
    sequence_batch, token_length, local_width = residual.shape
    row_count = sequence_batch * token_length
    members = lax.axis_size("rep")
    member = lax.axis_index("rep")
    units = gate_matrix.shape[1]
    share = units // members

    place = lax.broadcasted_iota(jnp.int32, (units, share), 0)
    wanted = lax.broadcasted_iota(jnp.int32, (units, share), 1) + member * share
    pick = (place == wanted).astype(bf16)

    def own_share(matrix):
        return jnp.dot(matrix.astype(bf16), pick, preferred_element_type=f32).astype(bf16)

    def own_scale(scale):
        return lax.dynamic_slice(scale, (member * share,), (share,))

    out_full = lax.all_gather(output_matrix.astype(bf16), "fs", axis=0, tiled=True)
    pair = jnp.concatenate([own_share(gate_matrix), own_share(up_matrix)], axis=1)
    pair_full = lax.all_gather(pair, "fs", axis=0, tiled=True)
    down_full = lax.all_gather(own_share(down_matrix), "fs", axis=0, tiled=True)

    normalized_rows = linear_attend(
        queries, key_matrix, value_matrix, decay_logodds, decay_surge, head_norm_gain
    ).reshape(row_count, -1)
    mix_terms = by_rows(normalized_rows, out_full)
    mix_total = lax.psum_scatter(
        mix_terms.astype(bf16), "tp", scatter_dimension=1, tiled=True
    ).astype(f32)
    own_rows = residual.reshape(row_count, local_width).astype(f32)
    updated = (own_rows + output_column_scale * mix_total).astype(bf16)
    group_rows = lax.all_gather(updated, "rep", axis=0, tiled=True)
    features = lax.all_gather(group_rows, "tp", axis=1, tiled=True)
    wide_rows = features.astype(f32)
    factor = lax.rsqrt(jnp.mean(wide_rows * wide_rows, axis=-1, keepdims=True) + epsilon)
    normin = (wide_rows * factor * premix_norm_gain).astype(bf16)
    both = jnp.dot(normin, pair_full, preferred_element_type=f32)
    gate_pre = both[:, :share] * own_scale(gate_column_scale)
    up_pre = both[:, share:] * own_scale(up_column_scale)
    hidden = (jax.nn.silu(gate_pre) * up_pre).astype(bf16)
    down_terms = by_rows(hidden, down_full).astype(bf16)
    down_half = lax.psum_scatter(down_terms, "tp", scatter_dimension=1, tiled=True)
    down_total = lax.psum_scatter(down_half, "rep", scatter_dimension=0, tiled=True).astype(f32)
    result = (updated.astype(f32) + down_column_scale * down_total).astype(bf16)
    return result.reshape(sequence_batch, token_length, local_width)


def solution(mesh):
    return jax.shard_map(
        body,
        mesh=mesh,
        in_specs=(
            P(("rep", "fs"), None, "tp"),
            P(("rep", "fs"), None, "tp"),
            P(("rep", "fs"), None, "tp"),
            P(("rep", "fs"), None, "tp"),
            P(("rep", "fs"), None, "tp"),
            P(("rep", "fs"), None, "tp"),
            P(),
            P("fs", "tp"),
            P("tp"),
            P(),
            P("fs", "tp"),
            P("tp"),
            P("fs", "tp"),
            P("tp"),
            P("fs", "tp"),
            P("tp"),
        ),
        out_specs=P(("rep", "fs"), None, "tp"),
        check_vma=False,
    )
```

time: 385 us -> 291 us (0.76)
  local copies, waits for them, and re-layouts: 50.7 us -> 3.29 us
  matrix products: 61.5 us -> 20.2 us
  other arithmetic: 34.1 us -> 10.8 us
  waiting for transfers between devices: 221 us -> 234 us
  Pallas kernels: 0 us -> 8.14 us
    reduce_scatter x2 -> x3, waiting for transfers between devices: 19.8 us -> 67.6 us  [the longest x1 47.2 us: body(): lax.psum_scatter(down_half, 'rep', scatter_dimension=0, tiled=True)]
    dot_general x21 -> x4, matrix products: 48.1 us -> 9.69 us  [the longest x1 6.29 us: body(): both = jnp.dot(normin, pair_full, preferred_element_type=f32)]
    all_gather x5, waiting for transfers between devices: 201 us -> 167 us  [the longest x1 47 us: body(): group_rows = lax.all_gather(updated, 'rep', axis=0, tiled=True)]
    rev x6 -> x0, local copies, waits for them, and re-layouts: 27.4 us -> none  [backwards(): return tensor[:, :, ::-1]]
    another operation x3 -> x0, local copies, waits for them, and re-layouts: 10.1 us -> none
    another operation x2 -> x0, other arithmetic: 8.77 us -> none  [one_direction(): running = jnp.cumsum(blocks(log_decay_values), axis=3)]
    pallas_call x0 -> x1, Pallas kernels: none -> 8.14 us  [linear_attend(): pl.pallas_call(attend_kernel, grid=(sequences, heads), in_specs=[spec(key...]
    transpose x5 -> x0, local copies, waits for them, and re-layouts: 7.07 us -> none  [the longest x4 4.59 us: split_heads(): jnp.transpose(tensor.astype(jnp.float32).reshape(sequence_batch, token_le...]
  transfers between devices with their start and end apart: 7 -> 8, of which waited for: 6 -> 8; matrix products, arithmetic and copies ran while one was open for 33% -> 6% of each run, Pallas kernels for 0% -> 3%
where the time goes in v1:
time: 291 us
  waiting for transfers between devices  234 us (80%)
  matrix products  20.2 us (7%)
  between operations  13.6 us (5%)
  other arithmetic  10.8 us (4%)
  Pallas kernels  8.14 us (3%)
  local copies, waits for them, and re-layouts  3.29 us (1%)
    reduce_scatter x1, waiting for transfers between devices, body(): lax.psum_scatter(down_half, 'rep', scatter_dimension=0, tiled=True)  47.2 us
    all_gather x1, waiting for transfers between devices, body(): group_rows = lax.all_gather(updated, 'rep', axis=0, tiled=True)  47 us
    all_gather x1, waiting for transfers between devices, body(): lax.all_gather(output_matrix.astype(bf16), 'fs', axis=0, tiled=True)  46.5 us
    all_gather x1, waiting for transfers between devices, body(): pair_full = lax.all_gather(pair, 'fs', axis=0, tiled=True)  41.3 us
    all_gather x1, waiting for transfers between devices, body(): down_full = lax.all_gather(own_share(down_matrix), 'fs', axis=0, tiled=True)  25 us
    reduce_scatter x1, waiting for transfers between devices, body(): lax.psum_scatter(down_terms, 'tp', scatter_dimension=1, tiled=True)  12 us
    dot_general x2, matrix products, by_rows(): lax.dot_general(left, right, (((1,), (1,)), ((), ())), preferred_element_...  10.5 us
    reduce_scatter x1, waiting for transfers between devices, body(): lax.psum_scatter(mix_terms.astype(bf16), 'tp', scatter_dimension=1, tiled...  8.46 us
  transfers between devices with their start and end apart: 8, of which 8 were waited for; matrix products, arithmetic and copies ran while one was open for 6% of the time, Pallas kernels for 3%

profile of v1, /device:TPU:0, one launch (start us, length us, event | category | flops | bytes accessed | tf_op | source)
XLA Modules:
  0.0 290.7 jit_solution(14091691424486481614)
XLA Ops:
  6.5 0.0 copy-start.4
  6.5 0.0 all-gather.6.cloned.1.call-start
  6.5 2.7 convert_element_type.69
  9.3 0.0 all-gather.6.cloned.1.call-update
  9.3 0.0 reduce-scatter.4.cloned.1.call-start
  9.4 0.0 copy-done.4
  9.4 0.8 copy.17.surge_ref
  10.2 8.1 %attend.1 = bf16[1,256,1024]{2,1,0:T(8,128)(2,1)} custom-call(bf16[1,256,1024]{2,1,0:T(8,128)(2,1)} %q_ref.1, bf16[1,256,1024]{2,1,0:T(8,128)(2,1)} %k_ref.1, bf16[1,256,1024]{2,1,0:T(8,128)(2,1)} %v_ref.1, f32[1,256,1024]{2,1,0:T(8,128)} %odds_ref.1, f32[1,256,4]{2,1,0:T(8,128)} %copy.17.surge_ref, f32[1,256]{1,0:T(1,128)} %bitcast.18), custom_call_target="tpu_custom_call" | custom-call | tf_op jit(solution)/shard_map/attend/pallas_call | solution.py:95
  18.3 0.0 copy-start.1
  18.3 0.0 copy-start.2
  18.3 46.5 %all-gather.6.cloned.1.call-done = bf16[2048,1024]{1,0:T(8,128)(2,1)} async-done(((bf16[512,1024]{1,0:T(8,128)(2,1)}), bf16[2048,1024]{1,0:T(8,128)(2,1)}) %all-gather.6.cloned.1.call-update) | async-done | bytes 4194320 | tf_op jit(solution)/shard_map/all_gather | solution.py:152
  64.8 4.6 %convolution_convert_fusion.1 = bf16[256,2048]{1,0:T(8,128)(2,1)} fusion(bf16[2048,1024]{1,0:T(8,128)(2,1)} %all-gather.6.cloned.1.call-done, bf16[1,256,1024]{2,1,0:T(8,128)(2,1)} %attend.1), kind=kOutput, calls=%fused_computation.9 | convolution fusion | flops 1074266112 | bytes 5767168 | tf_op jit(solution)/shard_map/dot_general | solution.py:114
  69.4 0.0 reduce-scatter.4.cloned.1.call-update
  69.4 0.0 copy-start.5
  69.4 0.0 all-gather.8.cloned.1.call-start
  69.5 8.5 %reduce-scatter.4.cloned.1.call-done = bf16[256,1024]{1,0:T(8,128)(2,1)} async-done(((bf16[256,2048]{1,0:T(8,128)(2,1)}), bf16[256,1024]{1,0:T(8,128)(2,1)}) %reduce-scatter.4.cloned.1.call-update) | async-done | bytes 524304 | tf_op jit(solution)/shard_map/reduce_scatter | solution.py:161
  77.9 0.0 copy-done.1
  77.9 0.0 copy-done.2
  77.9 2.0 fusion.52
  80.0 0.0 all-gather.8.cloned.1.call-update
  80.0 0.0 all-gather.10.cloned.1.call-start
  80.0 47.0 %all-gather.8.cloned.1.call-done = bf16[1024,1024]{1,0:T(8,128)(2,1)} async-done(((bf16[256,1024]{1,0:T(8,128)(2,1)}), bf16[1024,1024]{1,0:T(8,128)(2,1)}) %all-gather.8.cloned.1.call-update) | async-done | bytes 2097168 | tf_op jit(solution)/shard_map/all_gather | solution.py:166
  127.0 0.0 all-gather.10.cloned.1.call-update
  127.0 0.0 all-gather.12.cloned.1.call-start
  127.1 0.0 copy-start.6
  127.1 0.0 copy-done.5
  127.1 0.9 fusion.39
  128.0 0.9 copy-done.6
  128.9 0.0 copy-start.7
  128.9 0.9 fusion.44
  129.8 0.9 pad_maximum_fusion
  130.7 0.0 all-gather.12.cloned.1.call-update
  130.7 0.0 all-gather.14.cloned.1.call-start
  130.8 0.0 copy-done.7
  130.8 1.6 fusion.34
  132.4 0.0 all-gather.14.cloned.1.call-update
  132.4 0.0 copy-start.8
  132.4 0.0 reduce-scatter.6.cloned.1.call-start
  132.5 0.8 dynamic_slice.6
  133.3 0.8 dynamic_slice.7
  134.1 6.8 %all-gather.10.cloned.1.call-done = bf16[1024,2048]{1,0:T(8,128)(2,1)} async-done(((bf16[1024,1024]{1,0:T(8,128)(2,1)}), bf16[1024,2048]{1,0:T(8,128)(2,1)}) %all-gather.10.cloned.1.call-update) | async-done | bytes 4194320 | tf_op jit(solution)/shard_map/all_gather | solution.py:167
  140.9 3.1 %fusion = f32[1024]{0:T(1024)S(1)} fusion(bf16[1024,2048]{1,0:T(8,128)(2,1)} %all-gather.10.cloned.1.call-done), kind=kLoop, calls=%fused_computation.2 | loop fusion | flops 6290432 | bytes 4198400 | tf_op jit(solution)/shard_map/reduce_sum | solution.py:169
  144.0 41.3 %all-gather.12.cloned.1.call-done = bf16[2048,704]{0,1:T(8,128)(2,1)} async-done(((bf16[512,704]{0,1:T(8,128)(2,1)}), bf16[2048,704]{0,1:T(8,128)(2,1)}) %all-gather.12.cloned.1.call-update) | async-done | bytes 2883600 | tf_op jit(solution)/shard_map/all_gather | solution.py:154
  185.3 0.0 copy-done.8
  185.3 6.3 %fusion.3 = f32[1024,704]{0,1:T(8,128)S(1)} fusion(bf16[2048,704]{0,1:T(8,128)(2,1)} %all-gather.12.cloned.1.call-done, bf16[1024,2048]{1,0:T(8,128)(2,1)} %all-gather.10.cloned.1.call-done, f32[2048]{0:T(1024)S(1)} %copy-done.8, f32[1024]{0:T(1024)S(1)} %add_rsqrt_fusion), kind=kOutput, calls=%fused_computation.5 | convolution fusion | flops 2961178624 | bytes 9973760 | tf_op jit(solution)/shard_map/dot_general | solution.py:171
  191.6 25.0 %all-gather.14.cloned.1.call-done = bf16[2048,352]{0,1:T(8,128)(2,1)} async-done(((bf16[512,352]{0,1:T(8,128)(2,1)}), bf16[2048,352]{0,1:T(8,128)(2,1)}) %all-gather.14.cloned.1.call-update) | async-done | bytes 1441808 | tf_op jit(solution)/shard_map/all_gather | solution.py:155
  216.6 5.9 %convolution_convert_fusion = bf16[1024,2048]{1,0:T(8,128)(2,1)} fusion(bf16[2048,352]{0,1:T(8,128)(2,1)} %all-gather.14.cloned.1.call-done, f32[1024,704]{0,1:T(8,128)S(1)} %fusion.3, f32[352]{0:T(512)S(1)} %dynamic_slice.7, f32[352]{0:T(512)S(1)} %dynamic_slice.6), kind=kOutput, calls=%fused_computation.8 | convolution fusion | flops 1481375744 | bytes 8522496 | tf_op jit(solution)/shard_map/dot_general | solution.py:114
  222.6 0.0 copy-start
  222.6 0.0 copy-start.3
  222.6 0.0 reduce-scatter.6.cloned.1.call-update
  222.6 0.0 reduce-scatter.8.cloned.1.call-start
  222.7 12.0 %reduce-scatter.6.cloned.1.call-done = bf16[1024,1024]{1,0:T(8,128)(2,1)} async-done(((bf16[1024,2048]{1,0:T(8,128)(2,1)}), bf16[1024,1024]{1,0:T(8,128)(2,1)}) %reduce-scatter.6.cloned.1.call-update) | async-done | bytes 2097168 | tf_op jit(solution)/shard_map/reduce_scatter | solution.py:176
  234.6 0.0 reduce-scatter.8.cloned.1.call-update
  234.7 47.2 %reduce-scatter.8.cloned.1.call-done = bf16[256,1024]{1,0:T(8,128)(2,1)} async-done(((bf16[1024,1024]{1,0:T(8,128)(2,1)}), bf16[256,1024]{1,0:T(8,128)(2,1)}) %reduce-scatter.8.cloned.1.call-update) | async-done | bytes 524304 | tf_op jit(solution)/shard_map/reduce_scatter | solution.py:177
  281.9 0.0 copy-done
  281.9 0.0 copy-done.3
  281.9 2.0 fusion.57
  (2 shorter events, 0.0 us)
Async XLA Ops:
  6.5 2.8 copy-start.4
  6.5 58.2 %all-gather.6.cloned.1.call-start = ((), (), s32[]{:S(2)}) async-start(), calls=%async_computation.3 | async-start | bytes 5242880 | tf_op jit(solution)/shard_map/all_gather | solution.py:152
  9.3 68.6 %reduce-scatter.4.cloned.1.call-start = ((), (), s32[]{:S(2)}) async-start(), calls=%async_computation.4 | async-start | bytes 1572864 | tf_op jit(solution)/shard_map/reduce_scatter | solution.py:161
  18.3 59.6 %copy-start.1 = (bf16[1,256,1024]{2,1,0:T(8,128)(2,1)S(1)}, bf16[1,256,1024]{2,1,0:T(8,128)(2,1)}, u32[]{:S(2)}) copy-start(bf16[1,256,1024]{2,1,0:T(8,128)(2,1)} %param.16) | copy-start | bytes 1572868
  18.3 59.6 %copy-start.2 = (f32[1024]{0:T(1024)S(1)}, f32[1024]{0:T(1024)}, u32[]{:S(2)}) copy-start(f32[1024]{0:T(1024)} %param.24) | copy-start | bytes 12292
  69.4 57.7 %copy-start.5 = (f32[512,1408]{1,0:T(8,128)S(1)}, f32[512,1408]{1,0:T(8,128)}, u32[]{:S(2)}) copy-start(f32[512,1408]{1,0:T(8,128)} %param.28) | copy-start | bytes 8650756
  69.4 57.6 %all-gather.8.cloned.1.call-start = ((), (), s32[]{:S(2)}) async-start(), calls=%async_computation.5 | async-start | bytes 2621440 | tf_op jit(solution)/shard_map/all_gather | solution.py:166
  80.0 60.9 %all-gather.10.cloned.1.call-start = ((), (), s32[]{:S(2)}) async-start(), calls=%async_computation.6 | async-start | bytes 6291456 | tf_op jit(solution)/shard_map/all_gather | solution.py:167
  127.0 58.3 %all-gather.12.cloned.1.call-start = ((), (), s32[]{:S(2)}) async-start(), calls=%async_computation.7 | async-start | bytes 3604480 | tf_op jit(solution)/shard_map/all_gather | solution.py:154
  127.1 1.8 copy-start.6
  128.9 1.9 copy-start.7
  130.7 85.9 %all-gather.14.cloned.1.call-start = ((), (), s32[]{:S(2)}) async-start(), calls=%async_computation.8 | async-start | bytes 1802240 | tf_op jit(solution)/shard_map/all_gather | solution.py:155
  132.4 52.9 %copy-start.8 = (f32[2048]{0:T(1024)S(1)}, f32[2048]{0:T(1024)}, u32[]{:S(2)}) copy-start(f32[2048]{0:T(1024)} %param.25) | copy-start | bytes 24580
  132.4 102.2 %reduce-scatter.6.cloned.1.call-start = ((), (), s32[]{:S(2)}) async-start(), calls=%async_computation.9 | async-start | bytes 6291456 | tf_op jit(solution)/shard_map/reduce_scatter | solution.py:176
  222.6 59.3 %copy-start = (bf16[256,1024]{1,0:T(8,128)(2,1)S(1)}, bf16[256,1024]{1,0:T(8,128)(2,1)}, u32[]{:S(2)}) copy-start(bf16[256,1024]{1,0:T(8,128)(2,1)} %fusion.52) | copy-start | bytes 1572868
  222.6 59.3 %copy-start.3 = (f32[1024]{0:T(1024)S(1)}, f32[1024]{0:T(1024)}, u32[]{:S(2)}) copy-start(f32[1024]{0:T(1024)} %param.31) | copy-start | bytes 12292
  222.6 59.2 %reduce-scatter.8.cloned.1.call-start = ((), (), s32[]{:S(2)}) async-start(), calls=%async_computation.10 | async-start | bytes 2621440 | tf_op jit(solution)/shard_map/reduce_scatter | solution.py:177
Sparse Core Ops, SparseCore 0:
  9.4 55.2 all-gather.5
  69.5 8.3 reduce-scatter.3
  80.1 46.8 all-gather.7
  128.4 12.4 all-gather.9
  142.6 42.7 all-gather.11
  187.0 29.6 all-gather.13
  222.7 11.8 reduce-scatter.5
  236.9 44.8 reduce-scatter.7
